TPU v7x, 32 devices: a whole 2x2x4 slice. The times are simulated.
32 devices in a mesh: ep: 8 (over z, x), tp: 4 (over y, core).
Axes of the slice: x: 2, y: 2, z: 4, core: 2. Of those that a mesh axis runs over, the one named last changes fastest.
Arguments:
- queries: bfloat16 [6144, 1024], P('ep', 'tp'), may hold values from -6.5 to 6.5
- keys: bfloat16 [6144, 1024], P('ep', 'tp'), may hold values from -6.5 to 6.5
- values: bfloat16 [6144, 1024], P('ep', 'tp'), may hold values from -6 to 6
- cum_gate: float32 [6144, 16], P('ep', 'tp'), may hold values from -770 to 0, as said below
- head_gain: float32 [1024], P('tp'), may hold values from 0.1 to 1.9
- moe_in: bfloat16 [1024, 2048], P('ep'), may hold values from -6 to 6
- ffn_gain: float32 [2048], replicated, may hold values from 0.1 to 1.9
- routes: int32 [1024, 4], P('ep'), may hold values from 0 to 31, all different within a row; in each aligned block of 128 rows (0 to 127, 128 to 255, ...) at most 24 rows name the same one
- route_weight: float32 [1024, 4], P('ep'), may hold values from 0.2 to 1.2
- expert_gate: bfloat16 [32, 1024, 2048], P('ep', 'tp'), may hold values from -0.125 to 0.125
- expert_up: bfloat16 [32, 1024, 2048], P('ep', 'tp'), may hold values from -0.125 to 0.125
- expert_down: bfloat16 [32, 1024, 2048], P('ep', 'tp'), may hold values from -0.25 to 0.25
- shared_gate: bfloat16 [512, 2048], P('tp'), may hold values from -0.125 to 0.125
- shared_up: bfloat16 [512, 2048], P('tp'), may hold values from -0.125 to 0.125
- shared_down: bfloat16 [512, 2048], P('tp'), may hold values from -0.375 to 0.375
Outputs:
- mixed: bfloat16 [6144, 1024], P('ep', 'tp')
- expert_out: bfloat16 [1024, 2048], P('ep', 'tp')
Inputs may be any that keep to these rules, and one draw needn't show every extreme that they name: `routes`: in each aligned block of 128 rows (the tokens of one index of ep) no expert is named by more than 24 rows, a bound that some block reaches; a row names 4 different experts. Each head's cum_gate never rises from one position to the next.
All inputs are finite; a program needn't handle non-finite values.
Results may differ from a plain program's by a relative error of at most 0.019.
Values may be sent and summed in bfloat16 or wider, within the bound.
A program may use at most 128 MiB of HBM per device.

v0:
```python
import math

import jax
import jax.numpy as jnp
from jax import lax
from jax.sharding import PartitionSpec as P

NORM_EPSILON = 1e-06


def keep_same(state_pair):
    return state_pair


def attend(queries, keys, values, cum_gate, head_gain):
    row_count, head_width = queries.shape
    head_count = cum_gate.shape[1]
    head_size = head_width // head_count
    score_scale = head_size ** (-0.5)
    first_row = lax.axis_index("ep") * row_count
    last_row = first_row + row_count - 1
    query_heads = queries.reshape(row_count, head_count, head_size)
    query_pos = first_row + jnp.arange(row_count, dtype=jnp.int32)
    query_gate = cum_gate.T
    all_gates = lax.all_gather(cum_gate, "ep", axis=0, tiled=True)
    start_state = (
        jnp.full((head_count, row_count), -1e30, jnp.float32),
        jnp.zeros((row_count, head_count, head_size), jnp.float32),
    )
    key_piece = lax.all_gather(keys, "ep", axis=0, tiled=True)
    value_piece = lax.all_gather(values, "ep", axis=0, tiled=True)
    piece_len = key_piece.shape[0]
    block_len = math.gcd(piece_len, 512)

    def visit(block_num, state_pair):
        offset = block_num * block_len

        def update(pair_in):
            running, weighted = pair_in
            key_block = lax.dynamic_slice_in_dim(key_piece, offset, block_len, 0).reshape(
                block_len, head_count, head_size
            )
            value_block = lax.dynamic_slice_in_dim(value_piece, offset, block_len, 0).reshape(
                block_len, head_count, head_size
            )
            key_gate = lax.dynamic_slice_in_dim(all_gates, offset, block_len, 0).T
            key_pos = offset + jnp.arange(block_len, dtype=jnp.int32)
            scores = (
                jnp.einsum(
                    "qhd,khd->hqk", query_heads, key_block, preferred_element_type=jnp.float32
                )
                * score_scale
            )
            scores = scores + query_gate[:, :, None] - key_gate[:, None, :]
            scores = jnp.where(key_pos[None, None, :] <= query_pos[None, :, None], scores, -jnp.inf)
            new_peak = jnp.maximum(running, jnp.max(scores, axis=2))
            weights = jnp.exp(scores - new_peak[:, :, None]).astype(jnp.bfloat16)
            shrink = jnp.exp(running - new_peak).T
            weighted = weighted * shrink[:, :, None] + jnp.einsum(
                "hqk,khd->qhd", weights, value_block, preferred_element_type=jnp.float32
            )
            return (new_peak, weighted)

        return lax.cond(offset <= last_row, update, keep_same, state_pair)

    running, weighted = lax.fori_loop(0, piece_len // block_len, visit, start_state)
    mean_square = jnp.mean(weighted * weighted, axis=2, keepdims=True)
    normed = (
        weighted * lax.rsqrt(mean_square + NORM_EPSILON) * head_gain.reshape(head_count, head_size)
    )
    return normed.reshape(row_count, head_width).astype(jnp.bfloat16)


def slot_index(route_rows, experts, capacity):
    flat_routes = route_rows.reshape(-1)
    agreement_tally = (
        flat_routes[:, None] == jnp.arange(experts, dtype=jnp.int32)[None, :]
    ).astype(jnp.int32)
    earlier = jnp.sum((jnp.cumsum(agreement_tally, axis=0) - 1) * agreement_tally, axis=1)
    return flat_routes * capacity + earlier


def experts_half(
    moe_in,
    ffn_gain,
    routes,
    route_weight,
    expert_gate,
    expert_up,
    expert_down,
    shared_gate,
    shared_up,
    shared_down,
):
    tokens, model_width = moe_in.shape
    choose = routes.shape[1]
    per_group = expert_gate.shape[0]
    groups = lax.axis_size("ep")
    experts = per_group * groups
    capacity = max(2, 3 * tokens * choose // (2 * experts))
    slice_width = model_width // lax.axis_size("tp")
    source = moe_in.astype(jnp.float32)
    normed = (
        source
        * lax.rsqrt(jnp.mean(source * source, axis=1, keepdims=True) + NORM_EPSILON)
        * ffn_gain
    ).astype(jnp.bfloat16)
    shared_hidden = (
        jax.nn.silu(
            jnp.einsum("td,fd->tf", normed, shared_gate, preferred_element_type=jnp.float32)
        )
        * jnp.einsum("td,fd->tf", normed, shared_up, preferred_element_type=jnp.float32)
    ).astype(jnp.bfloat16)
    shared_term = jnp.dot(shared_hidden, shared_down, preferred_element_type=jnp.float32)
    slot_ids = slot_index(routes, experts, capacity)
    owner_row = (
        jnp.full((experts * capacity,), tokens, jnp.int32)
        .at[slot_ids]
        .set(jnp.arange(tokens * choose, dtype=jnp.int32) // choose)
    )
    padded = jnp.concatenate([normed, jnp.zeros((1, model_width), normed.dtype)], axis=0)
    own_columns = lax.dynamic_slice_in_dim(
        padded, lax.axis_index("tp") * slice_width, slice_width, 1
    )
    arrived = lax.all_to_all(own_columns[owner_row], "ep", split_axis=0, concat_axis=0, tiled=True)
    column_piece = lax.all_gather(arrived, "tp", axis=1, tiled=True)
    piece_len = column_piece.shape[1]
    arranged = column_piece.reshape(groups, per_group, capacity, piece_len)
    gate_value = jnp.einsum(
        "slcd,lfd->slcf", arranged, expert_gate, preferred_element_type=jnp.float32
    )
    up_value = jnp.einsum("slcd,lfd->slcf", arranged, expert_up, preferred_element_type=jnp.float32)
    hidden = (jax.nn.silu(gate_value) * up_value).astype(jnp.bfloat16)
    expert_term = jnp.einsum(
        "slcf,lfd->slcd", hidden, expert_down, preferred_element_type=jnp.float32
    ).reshape(groups * per_group * capacity, model_width)
    expert_sum, shared_sum = (
        lax.psum_scatter(
            expert_term.astype(jnp.bfloat16), "tp", scatter_dimension=1, tiled=True
        ).astype(jnp.float32),
        lax.psum_scatter(
            shared_term.astype(jnp.bfloat16), "tp", scatter_dimension=1, tiled=True
        ).astype(jnp.float32),
    )
    returned = lax.all_to_all(
        expert_sum.astype(jnp.bfloat16), "ep", split_axis=0, concat_axis=0, tiled=True
    )
    picked = returned[slot_ids].reshape(tokens, choose, slice_width).astype(jnp.float32)
    routed = jnp.sum(picked * route_weight[:, :, None], axis=1)
    return (shared_sum + routed).astype(jnp.bfloat16)


def on_device(
    queries,
    keys,
    values,
    cum_gate,
    head_gain,
    moe_in,
    ffn_gain,
    routes,
    route_weight,
    expert_gate,
    expert_up,
    expert_down,
    shared_gate,
    shared_up,
    shared_down,
):
    mixed = attend(queries, keys, values, cum_gate, head_gain)
    expert_out = experts_half(
        moe_in,
        ffn_gain,
        routes,
        route_weight,
        expert_gate,
        expert_up,
        expert_down,
        shared_gate,
        shared_up,
        shared_down,
    )
    return (mixed, expert_out)


def solution(mesh):
    in_specs = (
        P("ep", "tp"),
        P("ep", "tp"),
        P("ep", "tp"),
        P("ep", "tp"),
        P("tp"),
        P("ep", None),
        P(),
        P("ep", None),
        P("ep", None),
        P("ep", "tp", None),
        P("ep", "tp", None),
        P("ep", "tp", None),
        P("tp", None),
        P("tp", None),
        P("tp", None),
    )
    out_specs = (P("ep", "tp"), P("ep", "tp"))
    return jax.shard_map(
        on_device, mesh=mesh, in_specs=in_specs, out_specs=out_specs, check_vma=False
    )
```

profile of v0, /device:TPU:27, one launch (start us, length us, event | category | flops | bytes accessed | tf_op | source)
XLA Modules:
  0.0 309.0 jit_solution(3351411150945842040)
XLA Ops:
  12.8 2.4 scatter_custom_fusion
  16.6 2.7 gather_fusion
  19.3 23.3 %all_to_all.24 = bf16[8,96,512]{2,1,0:T(8,128)(2,1)} all-to-all(bf16[8,96,512]{2,1,0:T(8,128)(2,1)S(1)} %bitcast.100), channel_id=1, replica_groups=mesh['ep'=8,'tp'=4] {'ep'}, dimensions={0} | all-to-all | bytes 1572864 | tf_op jit(solution)/shard_map/all_to_all | solution.py:125
  42.6 30.3 %all-gather.8.cloned.1.call-done = bf16[768,2048]{1,0:T(8,128)(2,1)} async-done(((bf16[768,512]{1,0:T(8,128)(2,1)}), bf16[768,2048]{1,0:T(8,128)(2,1)}) %all-gather.8.cloned.1.call-update) | async-done | bytes 3145744 | tf_op jit(solution)/shard_map/all_gather | solution.py:126
  73.0 4.7 %fusion.23 = f32[8,4,24,256]{3,2,0,1:T(8,128)S(1)} fusion(bf16[4,256,2048]{2,1,0:T(8,128)(2,1)} %param.28, bf16[8,4,24,2048]{3,2,1,0:T(8,128)(2,1)} %bitcast.109), kind=kOutput, calls=%fused_computation.33 | convolution fusion | flops 805306368 | bytes 8126464 | tf_op jit(solution)/shard_map/slcd,lfd->slcf/dot_general | solution.py:129
  77.6 8.5 %fusion.18 = bf16[8,4,24,2048]{3,2,0,1:T(8,128)(2,1)} fusion(bf16[4,256,2048]{2,1,0:T(8,128)(2,1)} %param.30, bf16[4,256,2048]{2,1,0:T(8,128)(2,1)} %param.29, bf16[8,4,24,2048]{3,2,1,0:T(8,128)(2,1)} %bitcast.110, f32[8,4,24,256]{3,2,0,1:T(8,128)S(1)} %fusion.23), kind=kOutput, calls=%fused_computation.27 | convolution fusion | flops 1613365248 | bytes 15466496 | tf_op jit(solution)/shard_map/slcf,lfd->slcd/dot_general | solution.py:134
  86.1 4.1 %copy.32 = bf16[8,4,24,2048]{3,2,1,0:T(8,128)(2,1)} copy(bf16[8,4,24,2048]{3,2,0,1:T(8,128)(2,1)} %fusion.18) | data formatting | bytes 6291456 | tf_op jit(solution)/shard_map/convert_element_type | solution.py:139
  92.3 35.2 %reduce-scatter.5.cloned.1.call-done = bf16[768,512]{1,0:T(8,128)(2,1)} async-done(((bf16[768,2048]{1,0:T(8,128)(2,1)}), bf16[768,512]{1,0:T(8,128)(2,1)}) %reduce-scatter.5.cloned.1.call-update) | async-done | bytes 786448 | tf_op jit(solution)/shard_map/reduce_scatter | solution.py:138
  127.5 5.4 %all-to-all-start.1 = ((bf16[8,96,512]{2,1,0:T(8,128)(2,1)}), bf16[8,96,512]{2,1,0:T(8,128)(2,1)S(1)}, u32[]{:S(2)}, u32[]{:S(2)}) async-start(bf16[8,96,512]{2,1,0:T(8,128)(2,1)} %bitcast.103), calls=%async_computation.3 | async-start | bytes 1572864 | tf_op jit(solution)/shard_map/all_to_all | solution.py:145
  135.3 44.6 %all_gather.13 = f32[6144,4]{0,1:T(4,128)S(1)} all-gather(f32[768,4]{0,1:T(4,128)S(1)} %copy-done.6), channel_id=1, replica_groups=mesh['ep'=8,'tp'=4] {'ep'}, dimensions={0}, use_global_device_ids=true | all-gather | bytes 110592 | tf_op jit(solution)/shard_map/all_gather | solution.py:25
  179.9 46.6 %all-gather.6.cloned.1.call-done = bf16[6144,256]{0,1:T(8,128)(2,1)} async-done(((bf16[768,256]{0,1:T(8,128)(2,1)}), bf16[6144,256]{0,1:T(8,128)(2,1)}) %all-gather.6.cloned.1.call-update) | async-done | bytes 3145744 | tf_op jit(solution)/shard_map/all_gather | solution.py:31
  226.6 69.5 %while.16 = (s32[]{:T(128)}, f32[4,768]{1,0:T(4,128)S(1)}, f32[768,4,64]{0,2,1:T(8,128)S(1)}, s32[]{:T(128)}, bf16[6144,256]{0,1:T(8,128)(2,1)}, /*index=5*/bf16...) while((s32[]{:T(128)}, f32[4,768]{1,0:T(4,128)S(1)}, ...), condition=%wide.region_4.5_spmd.clone, body=%wide.region_0.4_spmd.clone.sunk | while | flops 420745472 | bytes 17461568 | solution.py:66
  226.7 5.8 %conditional.3 = ((f32[4,768]{1,0:T(4,128)S(1)}, f32[768,4,64]{0,2,1:T(8,128)S(1)})) conditional(s32[]{:T(128)} %convert_element_type.106, (f32[4,768]{1,0:T(4,128)S(1)}, f32[768,4,64]{0,2,1:T(8,128)S(1)}) %tuple.50, (s32[]{:T(128)}, s32[]{:T(128)}, bf16[6144,256]{0,1:T(8,128)(2,1)}, bf16[768,4,64]{0,2,1:T(8,128)(2,1)S(1)}, f32[4,768]{1,0:T(4,128)S(1)}, ...), branch_computations={%region_1.0_spmd, %region_2.3_spmd} | conditional | flops 420745472 | bytes 17458250 | solution.py:64
  230.0 2.4 fusion.6
  232.5 5.7 %conditional.3 = ((f32[4,768]{1,0:T(4,128)S(1)}, f32[768,4,64]{0,2,1:T(8,128)S(1)})) conditional(s32[]{:T(128)} %convert_element_type.106, (f32[4,768]{1,0:T(4,128)S(1)}, f32[768,4,64]{0,2,1:T(8,128)S(1)}) %tuple.50, (s32[]{:T(128)}, s32[]{:T(128)}, bf16[6144,256]{0,1:T(8,128)(2,1)}, bf16[768,4,64]{0,2,1:T(8,128)(2,1)S(1)}, f32[4,768]{1,0:T(4,128)S(1)}, ...), branch_computations={%region_1.0_spmd, %region_2.3_spmd} | conditional | flops 420745472 | bytes 17458250 | solution.py:64
  235.8 2.4 fusion.6
  238.3 5.7 %conditional.3 = ((f32[4,768]{1,0:T(4,128)S(1)}, f32[768,4,64]{0,2,1:T(8,128)S(1)})) conditional(s32[]{:T(128)} %convert_element_type.106, (f32[4,768]{1,0:T(4,128)S(1)}, f32[768,4,64]{0,2,1:T(8,128)S(1)}) %tuple.50, (s32[]{:T(128)}, s32[]{:T(128)}, bf16[6144,256]{0,1:T(8,128)(2,1)}, bf16[768,4,64]{0,2,1:T(8,128)(2,1)S(1)}, f32[4,768]{1,0:T(4,128)S(1)}, ...), branch_computations={%region_1.0_spmd, %region_2.3_spmd} | conditional | flops 420745472 | bytes 17458250 | solution.py:64
  241.6 2.4 fusion.6
  244.0 5.7 %conditional.3 = ((f32[4,768]{1,0:T(4,128)S(1)}, f32[768,4,64]{0,2,1:T(8,128)S(1)})) conditional(s32[]{:T(128)} %convert_element_type.106, (f32[4,768]{1,0:T(4,128)S(1)}, f32[768,4,64]{0,2,1:T(8,128)S(1)}) %tuple.50, (s32[]{:T(128)}, s32[]{:T(128)}, bf16[6144,256]{0,1:T(8,128)(2,1)}, bf16[768,4,64]{0,2,1:T(8,128)(2,1)S(1)}, f32[4,768]{1,0:T(4,128)S(1)}, ...), branch_computations={%region_1.0_spmd, %region_2.3_spmd} | conditional | flops 420745472 | bytes 17458250 | solution.py:64
  249.8 5.7 %conditional.3 = ((f32[4,768]{1,0:T(4,128)S(1)}, f32[768,4,64]{0,2,1:T(8,128)S(1)})) conditional(s32[]{:T(128)} %convert_element_type.106, (f32[4,768]{1,0:T(4,128)S(1)}, f32[768,4,64]{0,2,1:T(8,128)S(1)}) %tuple.50, (s32[]{:T(128)}, s32[]{:T(128)}, bf16[6144,256]{0,1:T(8,128)(2,1)}, bf16[768,4,64]{0,2,1:T(8,128)(2,1)S(1)}, f32[4,768]{1,0:T(4,128)S(1)}, ...), branch_computations={%region_1.0_spmd, %region_2.3_spmd} | conditional | flops 420745472 | bytes 17458250 | solution.py:64
  253.2 2.4 fusion.6
  255.6 5.7 %conditional.3 = ((f32[4,768]{1,0:T(4,128)S(1)}, f32[768,4,64]{0,2,1:T(8,128)S(1)})) conditional(s32[]{:T(128)} %convert_element_type.106, (f32[4,768]{1,0:T(4,128)S(1)}, f32[768,4,64]{0,2,1:T(8,128)S(1)}) %tuple.50, (s32[]{:T(128)}, s32[]{:T(128)}, bf16[6144,256]{0,1:T(8,128)(2,1)}, bf16[768,4,64]{0,2,1:T(8,128)(2,1)S(1)}, f32[4,768]{1,0:T(4,128)S(1)}, ...), branch_computations={%region_1.0_spmd, %region_2.3_spmd} | conditional | flops 420745472 | bytes 17458250 | solution.py:64
  261.4 5.7 %conditional.3 = ((f32[4,768]{1,0:T(4,128)S(1)}, f32[768,4,64]{0,2,1:T(8,128)S(1)})) conditional(s32[]{:T(128)} %convert_element_type.106, (f32[4,768]{1,0:T(4,128)S(1)}, f32[768,4,64]{0,2,1:T(8,128)S(1)}) %tuple.50, (s32[]{:T(128)}, s32[]{:T(128)}, bf16[6144,256]{0,1:T(8,128)(2,1)}, bf16[768,4,64]{0,2,1:T(8,128)(2,1)S(1)}, f32[4,768]{1,0:T(4,128)S(1)}, ...), branch_computations={%region_1.0_spmd, %region_2.3_spmd} | conditional | flops 420745472 | bytes 17458250 | solution.py:64
  264.8 2.4 fusion.6
  267.2 5.7 %conditional.3 = ((f32[4,768]{1,0:T(4,128)S(1)}, f32[768,4,64]{0,2,1:T(8,128)S(1)})) conditional(s32[]{:T(128)} %convert_element_type.106, (f32[4,768]{1,0:T(4,128)S(1)}, f32[768,4,64]{0,2,1:T(8,128)S(1)}) %tuple.50, (s32[]{:T(128)}, s32[]{:T(128)}, bf16[6144,256]{0,1:T(8,128)(2,1)}, bf16[768,4,64]{0,2,1:T(8,128)(2,1)S(1)}, f32[4,768]{1,0:T(4,128)S(1)}, ...), branch_computations={%region_1.0_spmd, %region_2.3_spmd} | conditional | flops 420745472 | bytes 17458250 | solution.py:64
  270.6 2.4 fusion.6
  273.0 5.7 %conditional.3 = ((f32[4,768]{1,0:T(4,128)S(1)}, f32[768,4,64]{0,2,1:T(8,128)S(1)})) conditional(s32[]{:T(128)} %convert_element_type.106, (f32[4,768]{1,0:T(4,128)S(1)}, f32[768,4,64]{0,2,1:T(8,128)S(1)}) %tuple.50, (s32[]{:T(128)}, s32[]{:T(128)}, bf16[6144,256]{0,1:T(8,128)(2,1)}, bf16[768,4,64]{0,2,1:T(8,128)(2,1)S(1)}, f32[4,768]{1,0:T(4,128)S(1)}, ...), branch_computations={%region_1.0_spmd, %region_2.3_spmd} | conditional | flops 420745472 | bytes 17458250 | solution.py:64
  276.4 2.4 fusion.6
  278.8 5.7 %conditional.3 = ((f32[4,768]{1,0:T(4,128)S(1)}, f32[768,4,64]{0,2,1:T(8,128)S(1)})) conditional(s32[]{:T(128)} %convert_element_type.106, (f32[4,768]{1,0:T(4,128)S(1)}, f32[768,4,64]{0,2,1:T(8,128)S(1)}) %tuple.50, (s32[]{:T(128)}, s32[]{:T(128)}, bf16[6144,256]{0,1:T(8,128)(2,1)}, bf16[768,4,64]{0,2,1:T(8,128)(2,1)S(1)}, f32[4,768]{1,0:T(4,128)S(1)}, ...), branch_computations={%region_1.0_spmd, %region_2.3_spmd} | conditional | flops 420745472 | bytes 17458250 | solution.py:64
  284.6 5.7 %conditional.3 = ((f32[4,768]{1,0:T(4,128)S(1)}, f32[768,4,64]{0,2,1:T(8,128)S(1)})) conditional(s32[]{:T(128)} %convert_element_type.106, (f32[4,768]{1,0:T(4,128)S(1)}, f32[768,4,64]{0,2,1:T(8,128)S(1)}) %tuple.50, (s32[]{:T(128)}, s32[]{:T(128)}, bf16[6144,256]{0,1:T(8,128)(2,1)}, bf16[768,4,64]{0,2,1:T(8,128)(2,1)S(1)}, f32[4,768]{1,0:T(4,128)S(1)}, ...), branch_computations={%region_1.0_spmd, %region_2.3_spmd} | conditional | flops 420745472 | bytes 17458250 | solution.py:64
  287.9 2.4 fusion.6
  290.4 5.7 %conditional.3 = ((f32[4,768]{1,0:T(4,128)S(1)}, f32[768,4,64]{0,2,1:T(8,128)S(1)})) conditional(s32[]{:T(128)} %convert_element_type.106, (f32[4,768]{1,0:T(4,128)S(1)}, f32[768,4,64]{0,2,1:T(8,128)S(1)}) %tuple.50, (s32[]{:T(128)}, s32[]{:T(128)}, bf16[6144,256]{0,1:T(8,128)(2,1)}, bf16[768,4,64]{0,2,1:T(8,128)(2,1)S(1)}, f32[4,768]{1,0:T(4,128)S(1)}, ...), branch_computations={%region_1.0_spmd, %region_2.3_spmd} | conditional | flops 420745472 | bytes 17458250 | solution.py:64
  (169 shorter events, 65.3 us)
Async XLA Ops:
  8.0 125.3 %copy-start = (bf16[128,2048]{1,0:T(8,128)(2,1)S(1)}, bf16[128,2048]{1,0:T(8,128)(2,1)}, u32[]{:S(2)}) copy-start(bf16[128,2048]{1,0:T(8,128)(2,1)} %param.33) | copy-start | bytes 1572868
  8.0 65.0 %all-gather.8.cloned.1.call-start = ((), (), s32[]{:S(2)}) async-start(), calls=%async_computation.7 | async-start | bytes 3932160 | tf_op jit(solution)/shard_map/all_gather | solution.py:126
  42.6 84.9 %reduce-scatter.5.cloned.1.call-start = ((), (), s32[]{:S(2)}) async-start(), calls=%async_computation.8 | async-start | bytes 3932160 | tf_op jit(solution)/shard_map/reduce_scatter | solution.py:138
  86.1 4.2 %copy-start.3 = (bf16[768,256]{1,0:T(8,128)(2,1)S(1)}, bf16[768,256]{1,0:T(8,128)(2,1)}, u32[]{:S(2)}) copy-start(bf16[768,256]{1,0:T(8,128)(2,1)} %param.20) | copy-start | bytes 1179652
  86.1 5.2 %copy-start.4 = (bf16[768,256]{1,0:T(8,128)(2,1)S(1)}, bf16[768,256]{1,0:T(8,128)(2,1)}, u32[]{:S(2)}) copy-start(bf16[768,256]{1,0:T(8,128)(2,1)} %param.21) | copy-start | bytes 1179652
  90.2 42.8 %copy-start.1 = (bf16[128,2048]{1,0:T(8,128)(2,1)S(1)}, bf16[128,2048]{1,0:T(8,128)(2,1)}, u32[]{:S(2)}) copy-start(bf16[128,2048]{1,0:T(8,128)(2,1)} %param.31) | copy-start | bytes 1572868
  90.2 43.1 %copy-start.2 = (bf16[128,2048]{1,0:T(8,128)(2,1)S(1)}, bf16[128,2048]{1,0:T(8,128)(2,1)}, u32[]{:S(2)}) copy-start(bf16[128,2048]{1,0:T(8,128)(2,1)} %param.32) | copy-start | bytes 1572868
  90.2 44.7 %copy-start.5 = (bf16[768,256]{1,0:T(8,128)(2,1)S(1)}, bf16[768,256]{1,0:T(8,128)(2,1)}, u32[]{:S(2)}) copy-start(bf16[768,256]{1,0:T(8,128)(2,1)} %param.19) | copy-start | bytes 1179652
  90.2 44.8 %copy-start.8 = (f32[256]{0:T(256)S(1)}, f32[256]{0:T(256)}, u32[]{:S(2)}) copy-start(f32[256]{0:T(256)} %param.23) | copy-start | bytes 3076
  90.3 44.9 %copy-start.7 = (f32[128,4]{0,1:T(4,128)S(1)}, f32[128,4]{0,1:T(4,128)}, u32[]{:S(2)}) copy-start(f32[128,4]{0,1:T(4,128)} %param.27) | copy-start | bytes 6148
  90.3 45.0 %copy-start.6 = (f32[768,4]{0,1:T(4,128)S(1)}, f32[768,4]{0,1:T(4,128)}, u32[]{:S(2)}) copy-start(f32[768,4]{0,1:T(4,128)} %param.22) | copy-start | bytes 36868
  90.3 89.6 %all-gather.4.cloned.1.call-start = ((), (), s32[]{:S(2)}) async-start(), calls=%async_computation.4 | async-start | bytes 3538944 | tf_op jit(solution)/shard_map/all_gather | solution.py:30
  91.3 135.3 %all-gather.6.cloned.1.call-start = ((), (), s32[]{:S(2)}) async-start(), calls=%async_computation.5 | async-start | bytes 3538944 | tf_op jit(solution)/shard_map/all_gather | solution.py:31
  127.5 169.8 %all-to-all-start.1 = ((bf16[8,96,512]{2,1,0:T(8,128)(2,1)}), bf16[8,96,512]{2,1,0:T(8,128)(2,1)S(1)}, u32[]{:S(2)}, u32[]{:S(2)}) async-start(bf16[8,96,512]{2,1,0:T(8,128)(2,1)} %bitcast.103), calls=%async_computation.3 | async-start | bytes 1572864 | tf_op jit(solution)/shard_map/all_to_all | solution.py:145
  132.9 167.4 %reduce-scatter.3.cloned.1.call-start = ((), (), s32[]{:S(2)}) async-start(), calls=%async_computation.6 | async-start | bytes 655360 | tf_op jit(solution)/shard_map/reduce_scatter | solution.py:141
Sparse Core Ops, SparseCore 0:
  42.7 30.1 all-gather.7
  90.3 37.1 reduce-scatter.4
  136.2 22.2 reduce-scatter.2
Sparse Core Ops, SparseCore 1:
  93.6 71.5 all-gather.3
  167.2 59.4 all-gather.5
where the time goes:
time: 310 us; the launch traced here: 309 us
  waiting for transfers between devices  112 us (36%)
  blocking collectives  67.9 us (22%)
  matrix products  66.4 us (21%)
  local copies, waits for them, and re-layouts  29.2 us (9%)
  between operations  15.5 us (5%)
  other arithmetic  10.8 us (3%)
  starting transfers between devices  5.61 us (2%)
    all_gather x1, waiting for transfers between devices, attend(): value_piece = lax.all_gather(values, 'ep', axis=0, tiled=True)  46.6 us
    all_gather x1, blocking collectives, attend(): all_gates = lax.all_gather(cum_gate, 'ep', axis=0, tiled=True)  44.6 us
    reduce_scatter x1, waiting for transfers between devices, experts_half(): lax.psum_scatter(expert_term.astype(jnp.bfloat16), 'tp', scatter_dimensio...  35.2 us
    all_gather x1, waiting for transfers between devices, experts_half(): column_piece = lax.all_gather(arrived, 'tp', axis=1, tiled=True)  30.3 us
    dot_general x12, matrix products, update(): jnp.einsum('hqk,khd->qhd', weights, value_block, preferred_element_type=j...  28.6 us
    all_to_all x1, blocking collectives, experts_half(): lax.all_to_all(own_columns[owner_row], 'ep', split_axis=0, concat_axis=0,...  23.3 us
    dot_general x12, matrix products, update(): jnp.einsum('qhd,khd->hqk', query_heads, key_block, preferred_element_type...  22.8 us
    dynamic_slice x12, local copies, waits for them, and re-layouts, update(): lax.dynamic_slice_in_dim(value_piece, offset, block_len, 0)  12.9 us
  transfers between devices with their start and end apart: 6, of which 3 were waited for; matrix products, arithmetic and copies ran while one was open for 25% of the time, Pallas kernels for 0%

commit v1 on v0

v1 whole, which is shorter than its diff:
```python
import functools
import math

import jax
import jax.numpy as jnp
from jax import lax
from jax.experimental import pallas as pl
from jax.experimental.pallas import tpu as pltpu
from jax.sharding import PartitionSpec as P

NORM_EPSILON = 1e-06
VMEM = pltpu.VMEM


def swap_halves(x):
    half = x.shape[1] // 2
    return jnp.concatenate([x[:, half:], x[:, :half]], axis=1)


def pack_kernel(splits, scale, q_ref, k_ref, v_ref, kv_ref, qp_ref):
    rows, width = q_ref.shape
    tile = rows // splits
    half = tile // 2
    low = lax.broadcasted_iota(jnp.int32, (rows, 128), 1) < 64
    low_half = low[:half]
    for head in range(width // 64):
        lanes = slice(head // 2 * 128, head // 2 * 128 + 128)
        kc, vc = k_ref[:, lanes], v_ref[:, lanes]
        qc = q_ref[:, lanes] * jnp.asarray(scale, q_ref.dtype)
        if head % 2 == 0:
            kv_ref[head] = jnp.where(low, kc, swap_halves(vc))
        else:
            kv_ref[head] = jnp.where(low, swap_halves(kc), vc)
        for part in range(splits):
            a = qc[part * tile : part * tile + half]
            b = qc[part * tile + half : (part + 1) * tile]
            if head % 2 == 0:
                packed = jnp.where(low_half, a, swap_halves(b))
            else:
                packed = jnp.where(low_half, swap_halves(a), b)
            qp_ref[head * splits + part] = packed


def flash_kernel(splits, packed, key_len, q_ref, kv_ref, gate_ref, gain_ref, out_ref):
    block = pl.program_id(0)
    part = lax.rem(lax.axis_index("ep"), splits)
    raw = q_ref[0]
    half = raw.shape[0]
    if packed:
        low = lax.broadcasted_iota(jnp.int32, raw.shape, 1) < 64
        zero = jnp.zeros_like(raw)
        query = jnp.concatenate(
            [jnp.where(low, raw, zero), jnp.where(low, swap_halves(raw), zero)], axis=0
        )
    else:
        query = raw
    rows = query.shape[0]

    def visit(step, state, masked):
        peak, weighted = state
        keys = kv_ref[pl.ds(pl.multiple_of(step * key_len, key_len), key_len), :]
        scores = lax.dot_general(
            query, keys, (((1,), (1,)), ((), ())), preferred_element_type=jnp.float32
        )
        scores = scores - gate_ref[step]
        if masked:
            row_pos = part * rows + lax.broadcasted_iota(jnp.int32, scores.shape, 0)
            key_pos = lax.broadcasted_iota(jnp.int32, scores.shape, 1)
            scores = jnp.where(key_pos <= row_pos, scores, -jnp.inf)
        new_peak = jnp.maximum(peak, jnp.max(scores, axis=1, keepdims=True))
        weights = jnp.exp(scores - new_peak).astype(jnp.bfloat16)
        weighted = weighted * jnp.exp(peak - new_peak) + jnp.dot(
            weights, keys, preferred_element_type=jnp.float32
        )
        return new_peak, weighted

    state = (jnp.full((rows, 1), -1e30, jnp.float32), jnp.zeros((rows, 128), jnp.float32))
    state = visit(block, state, True)
    state = lax.fori_loop(0, block, lambda step, s: visit(step, s, False), state)
    _, weighted = state
    high = lax.broadcasted_iota(jnp.int32, weighted.shape, 1) >= 64
    square = jnp.sum(jnp.where(high, weighted * weighted, 0.0), axis=1, keepdims=True) / 64
    normed = weighted * lax.rsqrt(square + NORM_EPSILON) * gain_ref[...]
    if packed:
        normed = jnp.where(high[:half], normed[half:], swap_halves(normed[:half]))
    out_ref[0] = normed.astype(out_ref.dtype)


def attend(queries, keys, values, cum_gate, head_gain):
    rows, width = queries.shape
    heads = cum_gate.shape[1]
    size = width // heads
    devices = lax.axis_size("ep")
    splits = devices // heads
    tile = rows // splits
    scale = size**-0.5
    packed = heads % 2 == 0 and (tile // 2) % 16 == 0
    send_rows = tile // 2 if packed else tile
    if packed:
        kv, qp = pl.pallas_call(
            functools.partial(pack_kernel, splits, scale),
            out_shape=(
                jax.ShapeDtypeStruct((heads, rows, 128), jnp.bfloat16),
                jax.ShapeDtypeStruct((devices, send_rows, 128), jnp.bfloat16),
            ),
            name="pack",
        )(queries, keys, values)
    else:
        kv = jnp.concatenate(
            [keys.reshape(rows, heads, size), values.reshape(rows, heads, size)], axis=2
        ).transpose(1, 0, 2)
        qs = (queries * jnp.asarray(scale, queries.dtype)).reshape(splits, tile, heads, size)
        qs = qs.transpose(2, 0, 1, 3).reshape(devices, tile, size)
        qp = jnp.concatenate([qs, jnp.zeros_like(qs)], axis=2)
    parcel = jnp.concatenate([jnp.repeat(kv, splits, axis=0), qp], axis=1)
    gates = jnp.repeat(cum_gate.T, splits, axis=0)
    all_gates = lax.all_to_all(gates, "ep", split_axis=0, concat_axis=0, tiled=True)
    got = lax.all_to_all(parcel, "ep", split_axis=0, concat_axis=0, tiled=True)
    kv_all = got[:, :rows].reshape(devices * rows, 128)
    q_all = got[:, rows:]
    head = lax.axis_index("ep") // splits
    gain = lax.dynamic_slice_in_dim(head_gain, head * size, size, 0)
    gain = jnp.concatenate([gain, gain])[None]
    flops = 2 * 2 * 128 * devices * (devices + 1) // 2 * tile * rows
    out = pl.pallas_call(
        functools.partial(flash_kernel, splits, packed, rows),
        grid=(devices,),
        in_specs=[
            pl.BlockSpec((1, send_rows, 128), lambda i: (i, 0, 0)),
            pl.BlockSpec(memory_space=VMEM),
            pl.BlockSpec(memory_space=VMEM),
            pl.BlockSpec(memory_space=VMEM),
        ],
        out_specs=pl.BlockSpec((1, send_rows, 128), lambda i: (i, 0, 0)),
        out_shape=jax.ShapeDtypeStruct((devices, send_rows, 128), jnp.bfloat16),
        cost_estimate=pl.CostEstimate(
            flops=flops, bytes_accessed=4 * devices * rows * 128, transcendentals=flops // 512
        ),
        compiler_params=pltpu.CompilerParams(vmem_limit_bytes=40 << 20),
        name="flash",
    )(q_all, kv_all, all_gates.reshape(devices, 1, rows), gain)
    back = lax.all_to_all(out, "ep", split_axis=0, concat_axis=0, tiled=True)
    if packed:
        back = back.reshape(heads, splits, tile // 2, 2, size).transpose(1, 3, 2, 0, 4)
    else:
        back = back[:, :, size:].reshape(heads, splits, tile, size).transpose(1, 2, 0, 3)
    return back.reshape(rows, width)


def experts_half(
    moe_in,
    ffn_gain,
    routes,
    route_weight,
    expert_gate,
    expert_up,
    expert_down,
    shared_gate,
    shared_up,
    shared_down,
):
    tokens, model_width = moe_in.shape
    per_group, hidden_width = expert_gate.shape[:2]
    groups = lax.axis_size("ep")
    parts = lax.axis_size("tp")
    here = lax.axis_index("ep")
    slice_width = model_width // parts
    total = groups * tokens
    own_columns = lax.dynamic_slice_in_dim(
        moe_in, lax.axis_index("tp") * slice_width, slice_width, 1
    )
    gathered = lax.all_gather(own_columns, ("ep", "tp"), axis=0, tiled=True)
    source = (
        gathered.reshape(groups, parts, tokens, slice_width)
        .transpose(0, 2, 1, 3)
        .reshape(total, model_width)
        .astype(jnp.float32)
    )
    normed = (
        source
        * lax.rsqrt(jnp.mean(source * source, axis=1, keepdims=True) + NORM_EPSILON)
        * ffn_gain
    ).astype(jnp.bfloat16)
    all_routes = lax.all_gather(routes, "ep", axis=0, tiled=True)
    all_weights = lax.all_gather(route_weight, "ep", axis=0, tiled=True)
    mine = here * per_group + jnp.arange(per_group, dtype=jnp.int32)
    share = jnp.sum(
        jnp.where(all_routes[:, :, None] == mine, all_weights[:, :, None], 0.0), axis=1
    )

    def product(left, right):
        return lax.dot_general(
            left, right, (((1,), (1,)), ((), ())), preferred_element_type=jnp.float32
        )

    gate_value = product(normed, expert_gate.reshape(-1, model_width))
    up_value = product(normed, expert_up.reshape(-1, model_width))
    hidden = jax.nn.silu(gate_value) * up_value
    hidden = hidden.reshape(total, per_group, hidden_width) * share[:, :, None]
    hidden = hidden.reshape(total, -1).astype(jnp.bfloat16)
    own = lax.dynamic_slice_in_dim(normed, here * tokens, tokens, 0)
    shared_hidden = (jax.nn.silu(product(own, shared_gate)) * product(own, shared_up)).astype(
        jnp.bfloat16
    )
    shared_term = jnp.dot(shared_hidden, shared_down, preferred_element_type=jnp.float32)
    term = jnp.dot(
        hidden, expert_down.reshape(-1, model_width), preferred_element_type=jnp.float32
    ).reshape(groups, tokens, model_width)
    is_own = (jnp.arange(groups, dtype=jnp.int32) == here)[:, None, None]
    term = (term + jnp.where(is_own, shared_term[None], 0.0)).astype(jnp.bfloat16)
    blocks = (
        term.reshape(groups, tokens, parts, slice_width)
        .transpose(0, 2, 1, 3)
        .reshape(groups * parts * tokens, slice_width)
    )
    return lax.psum_scatter(blocks, ("ep", "tp"), scatter_dimension=0, tiled=True)


def on_device(
    queries,
    keys,
    values,
    cum_gate,
    head_gain,
    moe_in,
    ffn_gain,
    routes,
    route_weight,
    expert_gate,
    expert_up,
    expert_down,
    shared_gate,
    shared_up,
    shared_down,
):
    expert_out = experts_half(
        moe_in,
        ffn_gain,
        routes,
        route_weight,
        expert_gate,
        expert_up,
        expert_down,
        shared_gate,
        shared_up,
        shared_down,
    )
    mixed = attend(queries, keys, values, cum_gate, head_gain)
    return (mixed, expert_out)


def solution(mesh):
    in_specs = (
        P("ep", "tp"),
        P("ep", "tp"),
        P("ep", "tp"),
        P("ep", "tp"),
        P("tp"),
        P("ep", None),
        P(),
        P("ep", None),
        P("ep", None),
        P("ep", "tp", None),
        P("ep", "tp", None),
        P("ep", "tp", None),
        P("tp", None),
        P("tp", None),
        P("tp", None),
    )
    out_specs = (P("ep", "tp"), P("ep", "tp"))
    return jax.shard_map(
        on_device, mesh=mesh, in_specs=in_specs, out_specs=out_specs, check_vma=False
    )
```

time: 310 us -> 302 us (0.974)
  the two profiles are of different devices: /device:TPU:27 before, /device:TPU:0 now
where the time goes in v1:
time: 302 us; the launch traced here: 301 us
  waiting for transfers between devices  90.7 us (30%)
  blocking collectives  68.7 us (23%)
  local copies, waits for them, and re-layouts  44.7 us (15%)
  Pallas kernels  31.5 us (10%)
  matrix products  26.6 us (9%)
  other arithmetic  14.5 us (5%)
  between operations  14.3 us (5%)
  starting transfers between devices  9.79 us (3%)
    all_to_all x1, waiting for transfers between devices, attend(): got = lax.all_to_all(parcel, 'ep', split_axis=0, concat_axis=0, tiled=True)  50.2 us
    reduce_scatter x1, waiting for transfers between devices, experts_half(): lax.psum_scatter(blocks, ('ep', 'tp'), scatter_dimension=0, tiled=True)  29.2 us
    pallas_call x1, Pallas kernels, attend(): pl.pallas_call(functools.partial(flash_kernel, splits, packed, rows), gri...  28.9 us
    all_gather x1, blocking collectives, experts_half(): all_routes = lax.all_gather(routes, 'ep', axis=0, tiled=True)  28.1 us
    all_gather x1, blocking collectives, experts_half(): all_weights = lax.all_gather(route_weight, 'ep', axis=0, tiled=True)  26.4 us
    dot_general x3, matrix products, product(): lax.dot_general(left, right, (((1,), (1,)), ((), ())), preferred_element_...  18.1 us
    all_to_all x1, blocking collectives, attend(): back = lax.all_to_all(out, 'ep', split_axis=0, concat_axis=0, tiled=True)  14.2 us
    unnamed x34, local copies, waits for them, and re-layouts  12.9 us
  transfers between devices with their start and end apart: 4, of which 4 were waited for; matrix products, arithmetic and copies ran while one was open for 5% of the time, Pallas kernels for 10%

profile of v1, /device:TPU:0, one launch (start us, length us, event | category | flops | bytes accessed | tf_op | source)
XLA Modules:
  0.0 300.8 jit_solution(2771459016561396435)
XLA Ops:
  7.2 1.6 constant_dynamic-slice_fusion
  9.6 28.1 %all_gather.10 = s32[1024,4]{0,1:T(4,128)S(1)} all-gather(s32[128,4]{0,1:T(4,128)} %param.22), channel_id=1, replica_groups=mesh['ep'=8,'tp'=4] {'ep'}, dimensions={0}, use_global_device_ids=true | all-gather | bytes 18432 | tf_op jit(solution)/shard_map/all_gather | solution.py:184
  37.8 26.4 %all_gather.11 = f32[1024,4]{0,1:T(4,128)S(1)} all-gather(f32[128,4]{0,1:T(4,128)} %param.23), channel_id=1, replica_groups=mesh['ep'=8,'tp'=4] {'ep'}, dimensions={0}, use_global_device_ids=true | all-gather | bytes 18432 | tf_op jit(solution)/shard_map/all_gather | solution.py:185
  64.5 1.2 mul.88
  65.7 2.9 copy.39
  68.7 7.3 %all-gather.2.cloned.1.call-done = bf16[4096,512]{1,0:T(8,128)(2,1)} async-done(((bf16[128,512]{1,0:T(8,128)(2,1)}), bf16[4096,512]{1,0:T(8,128)(2,1)}) %all-gather.2.cloned.1.call-update) | async-done | bytes 4194320 | tf_op jit(solution)/shard_map/all_gather | solution.py:172
  76.0 3.2 %multiply_reduce_fusion = f32[8,128]{1,0:T(8,128)S(1)} fusion(bf16[8,4,128,512]{3,2,1,0:T(8,128)(2,1)} %bitcast.54), kind=kLoop, calls=%fused_computation.3 | loop fusion | flops 6290432 | bytes 4198400 | tf_op jit(solution)/shard_map/reduce_sum | solution.py:181
  79.4 4.4 %bitcast_convert_fusion = f32[8,4,128,512]{3,2,1,0:T(8,128)} fusion(bf16[4096,512]{1,0:T(8,128)(2,1)S(1)} %copy-done.2), kind=kLoop, calls=%fused_computation.30 | loop fusion | flops 2097152 | bytes 12582912 | tf_op jit(solution)/shard_map/convert_element_type | solution.py:177
  83.8 10.0 %copy.31 = f32[8,4,128,512]{2,0,3,1:T(8,128)} copy(f32[8,4,128,512]{3,2,1,0:T(8,128)} %bitcast_convert_fusion) | data formatting | bytes 16777216 | tf_op jit(solution)/shard_map/convert_element_type | solution.py:177
  93.8 5.7 %copy.52 = f32[256,8,8,128]{3,1,2,0:T(8,128)S(1)} copy(f32[256,8,8,128]{3,2,1,0:T(8,128)} %bitcast.51) | data formatting | bytes 16777216
  99.6 4.2 %multiply_convert_fusion = bf16[8,4,128,512]{2,0,3,1:T(8,128)(2,1)S(1)} fusion(f32[8,4,128,512]{2,0,3,1:T(8,128)S(1)} %bitcast.53, f32[4,512]{1,0:T(4,128)S(1)} %mul.81, f32[8,128]{1,0:T(8,128)S(1)} %get-tuple-element.10), kind=kLoop, calls=%fused_computation.2 | loop fusion | flops 6291456 | bytes 12595200 | tf_op jit(solution)/shard_map/convert.4
  103.9 0.8 copy-done.10
  104.7 6.1 %fusion = f32[1024,1024]{1,0:T(8,128)} fusion(bf16[1024,2048]{1,0:T(8,128)(2,1)S(1)} %bitcast.66, bf16[256,8,8,128]{3,2,1,0:T(8,128)(2,1)S(1)} %bitcast.61), kind=kOutput, calls=%fused_computation.4 | convolution fusion | flops 4294967296 | bytes 12582912 | tf_op jit(solution)/shard_map/dot_general | solution.py:192
  111.6 2.5 fusion.9
  114.1 11.3 %multiply_convert_fusion.1 = bf16[1024,1024]{1,0:T(8,128)(2,1)S(1)} fusion(f32[1024,1024]{1,0:T(8,128)} %bitcast.63, f32[1024,1024]{1,0:T(8,128)} %fusion, bf16[1024,2048]{1,0:T(8,128)(2,1)} %bitcast.67, bf16[256,8,8,128]{3,2,1,0:T(8,128)(2,1)} %bitcast.62), kind=kOutput, calls=%fused_computation.8 | convolution fusion | flops 4302307328 | bytes 18874368 | tf_op jit(solution)/shard_map/dot_general | solution.py:192
  125.4 6.1 %add_convert_fusion = bf16[8,128,2048]{2,1,0:T(8,128)(2,1)} fusion(f32[128,2048]{1,0:T(8,128)S(1)} %fusion.9, pred[8]{0:T(512)(128)(4,1)S(1)} %iota_compare_fusion, bf16[8,128,1024]{2,1,0:T(8,128)(2,1)S(1)} %bitcast.69, bf16[1024,2048,1]{1,0,2:T(8,128)(2,1)S(1)} %bitcast.68), kind=kOutput, calls=%fused_computation.1 | convolution fusion | flops 4301258752 | bytes 11534344 | tf_op jit(solution)/shard_map/dot_general | solution.py:206
  131.4 7.9 %reshape.108 = bf16[8,128,4,512]{3,2,1,0:T(4,128)(2,1)} reshape(bf16[8,128,2048]{2,1,0:T(8,128)(2,1)} %add_convert_fusion) | data formatting | bytes 8388608 | tf_op jit(solution)/shard_map/reshape | solution.py:212
  139.3 5.2 %copy.34 = bf16[8,4,128,512]{3,2,1,0:T(8,128)(2,1)} copy(bf16[8,4,128,512]{3,1,2,0:T(4,128)(2,1)} %bitcast.57) | data formatting | bytes 8388608 | tf_op jit(solution)/shard_map/transpose | solution.py:213
  144.6 2.6 pack.1
  147.2 1.4 broadcast_in_dim.49
  148.5 2.5 pad_maximum_fusion
  151.0 4.0 %all-to-all-start = ((bf16[8,960,128]{2,1,0:T(8,128)(2,1)}), bf16[8,960,128]{2,1,0:T(8,128)(2,1)S(1)}, u32[]{:S(2)}, u32[]{:S(2)}) async-start(bf16[8,960,128]{2,1,0:T(8,128)(2,1)} %pad_maximum_fusion), calls=%async_computation | async-start | bytes 3932160 | tf_op jit(solution)/shard_map/all_to_all | solution.py:118
  155.8 50.2 %all-to-all-done = bf16[8,960,128]{2,1,0:T(8,128)(2,1)S(1)} async-done(((bf16[8,960,128]{2,1,0:T(8,128)(2,1)}), bf16[8,960,128]{2,1,0:T(8,128)(2,1)S(1)}, u32[]{:S(2)}, u32[]{:S(2)}) %all-to-all-start) | async-done | bytes 1966112 | tf_op jit(solution)/shard_map/all_to_all | solution.py:118
  206.0 1.3 copy-done.4
  207.2 5.7 %all-to-all-start.1 = ((f32[8,1,768]{2,1,0:T(1,128)}), f32[8,1,768]{2,1,0:T(1,128)S(1)}, u32[]{:S(2)}, u32[]{:S(2)}) async-start(f32[8,1,768]{2,1,0:T(1,128)} %all_to_all.13), calls=%async_computation.1 | async-start | bytes 49152 | tf_op jit(solution)/shard_map/all_to_all | solution.py:117
  213.0 1.5 slice.9
  214.5 1.0 slice.8.q_ref
  215.6 4.0 %all-to-all-done.1.gate_ref = f32[8,1,768]{2,1,0:T(1,128)S(1)} async-done(((f32[8,1,768]{2,1,0:T(1,128)}), f32[8,1,768]{2,1,0:T(1,128)S(1)}, u32[]{:S(2)}, u32[]{:S(2)}) %all-to-all-start.1) | async-done | bytes 24608 | tf_op jit(solution)/shard_map/all_to_all | solution.py:117
  219.6 28.9 %flash.1 = bf16[8,192,128]{2,1,0:T(8,128)(2,1)S(1)} custom-call(bf16[8,192,128]{2,1,0:T(8,128)(2,1)S(1)} %slice.8.q_ref, bf16[6144,128]{1,0:T(8,128)(2,1)S(1)} %bitcast.50, f32[8,1,768]{2,1,0:T(1,128)S(1)} %all-to-all-done.1.gate_ref, f32[1,128]{1,0:T(1,128)S(1)} %maximum_bitcast_fusion.gain_ref), custom_call_target="tpu_custom_call" | custom-call | flops 5435817984 | bytes 3145728 | tf_op jit(solution)/shard_map/flash/pallas_call | solution.py:125
  248.5 14.2 %all_to_all.19 = bf16[8,192,128]{2,1,0:T(8,128)(2,1)S(1)} all-to-all(bf16[8,192,128]{2,1,0:T(8,128)(2,1)S(1)} %flash.1), channel_id=1, replica_groups=mesh['ep'=8,'tp'=4] {'ep'}, dimensions={0} | all-to-all | bytes 786432 | tf_op jit(solution)/shard_map/all_to_all | solution.py:142
  263.5 1.2 reshape.114
  264.8 29.2 %reduce-scatter.2.cloned.1.call-done = bf16[128,512]{1,0:T(8,128)(2,1)} async-done(((bf16[4096,512]{1,0:T(8,128)(2,1)}), bf16[128,512]{1,0:T(8,128)(2,1)}) %reduce-scatter.2.cloned.1.call-update) | async-done | bytes 131088 | tf_op jit(solution)/shard_map/reduce_scatter | solution.py:216
  (47 shorter events, 3.8 us)
Async XLA Ops:
  7.2 104.4 %copy-start = (bf16[128,2048]{1,0:T(8,128)(2,1)S(1)}, bf16[128,2048]{1,0:T(8,128)(2,1)}, u32[]{:S(2)}) copy-start(bf16[128,2048]{1,0:T(8,128)(2,1)} %param.29) | copy-start | bytes 1572868
  7.2 68.8 %all-gather.2.cloned.1.call-start = ((), (), s32[]{:S(2)}) async-start(), calls=%async_computation.4 | async-start | bytes 4325376 | tf_op jit(solution)/shard_map/all_gather | solution.py:172
  8.9 285.1 %reduce-scatter.2.cloned.1.call-start = ((), (), s32[]{:S(2)}) async-start(), calls=%async_computation.5 | async-start | bytes 4325376 | tf_op jit(solution)/shard_map/reduce_scatter | solution.py:216
  76.0 3.4 %copy-start.2 = (bf16[4096,512]{1,0:T(8,128)(2,1)S(1)}, bf16[4096,512]{1,0:T(8,128)(2,1)}, u32[]{:S(2)}) copy-start(bf16[4096,512]{1,0:T(8,128)(2,1)} %all-gather.2.cloned.1.call-done) | copy-start | bytes 12582916
  93.8 5.8 %slice-start = ((s8[8388608]{0:T(1024)(128)(4,1)}), s8[4194304]{0:T(1024)(128)(4,1)S(1)}, s32[]{:S(2)}) async-start(s8[8388608]{0:T(1024)(128)(4,1)} %bitcast.52), calls=%async_computation.6 | async-start | bytes 8388608
  93.8 5.9 %slice-start.1 = ((s8[8388608]{0:T(1024)(128)(4,1)}), s8[4194304]{0:T(1024)(128)(4,1)S(1)}, s32[]{:S(2)}) async-start(s8[8388608]{0:T(1024)(128)(4,1)} %bitcast.52), calls=%async_computation.7 | async-start | bytes 8388608
  99.5 11.4 %copy-start.3 = (f32[256,8,8,128]{3,1,2,0:T(8,128)}, f32[256,8,8,128]{3,1,2,0:T(8,128)S(1)}, u32[]{:S(2)}) copy-start(f32[256,8,8,128]{3,1,2,0:T(8,128)S(1)} %copy.52) | copy-start | bytes 25165828
  99.6 5.1 %copy-start.10 = (bf16[4,256,2048]{2,1,0:T(8,128)(2,1)S(1)}, bf16[4,256,2048]{2,1,0:T(8,128)(2,1)}, u32[]{:S(2)}) copy-start(bf16[4,256,2048]{2,1,0:T(8,128)(2,1)} %param.25) | copy-start | bytes 12582916
  103.9 7.0 %copy-start.5 = (bf16[8,4,128,512]{2,0,3,1:T(8,128)(2,1)}, bf16[8,4,128,512]{2,0,3,1:T(8,128)(2,1)S(1)}, u32[]{:S(2)}) copy-start(bf16[8,4,128,512]{2,0,3,1:T(8,128)(2,1)S(1)} %multiply_convert_fusion) | copy-start | bytes 12582916
  104.7 6.2 %copy-start.6 = (bf16[128,2048]{1,0:T(8,128)(2,1)S(1)}, bf16[128,2048]{1,0:T(8,128)(2,1)}, u32[]{:S(2)}) copy-start(bf16[128,2048]{1,0:T(8,128)(2,1)} %param.27) | copy-start | bytes 1572868
  104.7 6.2 %copy-start.8 = (f32[2048]{0:T(1024)S(1)}, f32[2048]{0:T(1024)}, u32[]{:S(2)}) copy-start(f32[2048]{0:T(1024)} %param.21) | copy-start | bytes 24580
  104.7 6.9 %copy-start.7 = (bf16[128,2048]{1,0:T(8,128)(2,1)S(1)}, bf16[128,2048]{1,0:T(8,128)(2,1)}, u32[]{:S(2)}) copy-start(bf16[128,2048]{1,0:T(8,128)(2,1)} %param.28) | copy-start | bytes 1572868
  114.1 11.3 %copy-start.11 = (bf16[4,256,2048]{2,1,0:T(8,128)(2,1)S(1)}, bf16[4,256,2048]{2,1,0:T(8,128)(2,1)}, u32[]{:S(2)}) copy-start(bf16[4,256,2048]{2,1,0:T(8,128)(2,1)} %param.26) | copy-start | bytes 12582916
  148.5 6.5 %copy-start.9 = (f32[768,4]{0,1:T(4,128)S(1)}, f32[768,4]{0,1:T(4,128)}, u32[]{:S(2)}) copy-start(f32[768,4]{0,1:T(4,128)} %param.18) | copy-start | bytes 36868
  148.5 7.2 %copy-start.12 = (f32[256]{0:T(256)S(1)}, f32[256]{0:T(256)}, u32[]{:S(2)}) copy-start(f32[256]{0:T(256)} %param.19) | copy-start | bytes 3076
  151.0 54.9 %all-to-all-start = ((bf16[8,960,128]{2,1,0:T(8,128)(2,1)}), bf16[8,960,128]{2,1,0:T(8,128)(2,1)S(1)}, u32[]{:S(2)}, u32[]{:S(2)}) async-start(bf16[8,960,128]{2,1,0:T(8,128)(2,1)} %pad_maximum_fusion), calls=%async_computation | async-start | bytes 3932160 | tf_op jit(solution)/shard_map/all_to_all | solution.py:118
  206.0 1.3 copy-start.4
  207.2 12.3 %all-to-all-start.1 = ((f32[8,1,768]{2,1,0:T(1,128)}), f32[8,1,768]{2,1,0:T(1,128)S(1)}, u32[]{:S(2)}, u32[]{:S(2)}) async-start(f32[8,1,768]{2,1,0:T(1,128)} %all_to_all.13), calls=%async_computation.1 | async-start | bytes 49152 | tf_op jit(solution)/shard_map/all_to_all | solution.py:117
  219.6 74.4 %copy-start.1 = (bf16[128,2048]{1,0:T(8,128)(2,1)S(1)}, bf16[128,2048]{1,0:T(8,128)(2,1)}, u32[]{:S(2)}) copy-start(bf16[128,2048]{1,0:T(8,128)(2,1)} %param.29) | copy-start | bytes 1572868
Sparse Core Ops, SparseCore 0:
  11.4 64.4 all-gather.1
  144.7 149.2 reduce-scatter.1

commit v2 on v1

--- a/solution.py
+++ b/solution.py
@@ -86,9 +86,22 @@
     out_ref[0] = normed.astype(out_ref.dtype)
 
 
-def attend(queries, keys, values, cum_gate, head_gain):
+def trade_small(cum_gate, routes, route_weight):
+    rows, heads = cum_gate.shape
+    devices = lax.axis_size("ep")
+    tokens, choose = routes.shape
+    gates = jnp.repeat(cum_gate.T, devices // heads, axis=0)
+    named = jnp.concatenate([routes.astype(jnp.float32).reshape(-1), route_weight.reshape(-1)])
+    small = jnp.concatenate([gates, jnp.broadcast_to(named, (devices, named.size))], axis=1)
+    small = lax.all_to_all(small, "ep", split_axis=0, concat_axis=0, tiled=True)
+    count = tokens * choose
+    all_routes = small[:, rows : rows + count].astype(jnp.int32).reshape(-1, choose)
+    all_weights = small[:, rows + count :].reshape(-1, choose)
+    return small[:, :rows], all_routes, all_weights
+
+
+def trade_rows(queries, keys, values, heads):
     rows, width = queries.shape
-    heads = cum_gate.shape[1]
     size = width // heads
     devices = lax.axis_size("ep")
     splits = devices // heads
@@ -113,9 +126,16 @@
         qs = qs.transpose(2, 0, 1, 3).reshape(devices, tile, size)
         qp = jnp.concatenate([qs, jnp.zeros_like(qs)], axis=2)
     parcel = jnp.concatenate([jnp.repeat(kv, splits, axis=0), qp], axis=1)
-    gates = jnp.repeat(cum_gate.T, splits, axis=0)
-    all_gates = lax.all_to_all(gates, "ep", split_axis=0, concat_axis=0, tiled=True)
-    got = lax.all_to_all(parcel, "ep", split_axis=0, concat_axis=0, tiled=True)
+    return lax.all_to_all(parcel, "ep", split_axis=0, concat_axis=0, tiled=True), packed
+
+
+def attend(got, packed, rows, all_gates, heads, head_gain):
+    devices, parcel_rows, _ = got.shape
+    width = head_gain.shape[0]
+    size = width // heads
+    splits = devices // heads
+    tile = rows // splits
+    send_rows = parcel_rows - rows
     kv_all = got[:, :rows].reshape(devices * rows, 128)
     q_all = got[:, rows:]
     head = lax.axis_index("ep") // splits
@@ -147,11 +167,82 @@
     return back.reshape(rows, width)
 
 
-def experts_half(
-    moe_in,
+def norm_kernel(x_ref, gain_ref, out_ref):
+    parts, _, width = x_ref.shape
+    pieces = [x_ref[part].astype(jnp.float32) for part in range(parts)]
+    square = sum(jnp.sum(p * p, axis=1, keepdims=True) for p in pieces) / (parts * width)
+    factor = lax.rsqrt(square + NORM_EPSILON)
+    for part, piece in enumerate(pieces):
+        lanes = slice(part * width, (part + 1) * width)
+        out_ref[:, lanes] = (piece * factor * gain_ref[:, lanes]).astype(out_ref.dtype)
+
+
+def gated(rows, gate, up):
+    dims = (((1,), (1,)), ((), ()))
+    gate_value = lax.dot_general(rows, gate, dims, preferred_element_type=jnp.float32)
+    up_value = lax.dot_general(rows, up, dims, preferred_element_type=jnp.float32)
+    return gate_value / (1.0 + jnp.exp(-gate_value)) * up_value
+
+
+def hidden_kernel(
+    x_ref, routes_ref, weight_ref, gate_ref, up_ref, sgate_ref, sup_ref, hid_ref, shid_ref
+):
+    expert = pl.program_id(0)
+    here = lax.axis_index("ep")
+    tokens = shid_ref.shape[0]
+    number = here * pl.num_programs(0) + expert
+    chunk = min(256, x_ref.shape[0])
+
+    @pl.loop(0, x_ref.shape[0] // chunk)
+    def _(step):
+        rows = pl.ds(pl.multiple_of(step * chunk, chunk), chunk)
+        share = jnp.sum(
+            jnp.where(routes_ref[rows, :] == number, weight_ref[rows, :], 0.0),
+            axis=1,
+            keepdims=True,
+        )
+        value = gated(x_ref[rows, :], gate_ref[0], up_ref[0])
+        hid_ref[0, rows, :] = (value * share).astype(hid_ref.dtype)
+
+    @pl.when(expert == 0)
+    def _():
+        own = x_ref[pl.ds(pl.multiple_of(here * tokens, tokens), tokens), :]
+        shid_ref[...] = gated(own, sgate_ref[...], sup_ref[...]).astype(shid_ref.dtype)
+
+
+def down_kernel(hid_ref, shid_ref, down_ref, sdown_ref, out_ref):
+    tokens = shid_ref.shape[0]
+    here = lax.axis_index("ep")
+    per_group = down_ref.shape[0]
+
+    @pl.loop(0, hid_ref.shape[1] // tokens)
+    def _(step):
+        rows = pl.ds(pl.multiple_of(step * tokens, tokens), tokens)
+        term = sum(
+            jnp.dot(hid_ref[expert, rows, :], down_ref[expert], preferred_element_type=jnp.float32)
+            for expert in range(per_group)
+        )
+        out_ref[0, rows, :] = term.astype(out_ref.dtype)
+
+        @pl.when(step == here)
+        def _():
+            extra = jnp.dot(shid_ref[...], sdown_ref[...], preferred_element_type=jnp.float32)
+            out_ref[0, rows, :] = (term + extra).astype(out_ref.dtype)
+
+
+def gather_tokens(moe_in):
+    slice_width = moe_in.shape[1] // lax.axis_size("tp")
+    own_columns = lax.dynamic_slice_in_dim(
+        moe_in, lax.axis_index("tp") * slice_width, slice_width, 1
+    )
+    return lax.all_gather(own_columns, ("ep", "tp"), axis=0)
+
+
+def expert_terms(
+    gathered,
     ffn_gain,
-    routes,
-    route_weight,
+    all_routes,
+    all_weights,
     expert_gate,
     expert_up,
     expert_down,
@@ -159,61 +250,79 @@
     shared_up,
     shared_down,
 ):
-    tokens, model_width = moe_in.shape
+    tokens = gathered.shape[1]
+    model_width = ffn_gain.shape[0]
     per_group, hidden_width = expert_gate.shape[:2]
+    shared_width = shared_gate.shape[0]
     groups = lax.axis_size("ep")
     parts = lax.axis_size("tp")
-    here = lax.axis_index("ep")
     slice_width = model_width // parts
     total = groups * tokens
-    own_columns = lax.dynamic_slice_in_dim(
-        moe_in, lax.axis_index("tp") * slice_width, slice_width, 1
-    )
-    gathered = lax.all_gather(own_columns, ("ep", "tp"), axis=0, tiled=True)
-    source = (
-        gathered.reshape(groups, parts, tokens, slice_width)
-        .transpose(0, 2, 1, 3)
-        .reshape(total, model_width)
-        .astype(jnp.float32)
-    )
-    normed = (
-        source
-        * lax.rsqrt(jnp.mean(source * source, axis=1, keepdims=True) + NORM_EPSILON)
-        * ffn_gain
-    ).astype(jnp.bfloat16)
-    all_routes = lax.all_gather(routes, "ep", axis=0, tiled=True)
-    all_weights = lax.all_gather(route_weight, "ep", axis=0, tiled=True)
-    mine = here * per_group + jnp.arange(per_group, dtype=jnp.int32)
-    share = jnp.sum(
-        jnp.where(all_routes[:, :, None] == mine, all_weights[:, :, None], 0.0), axis=1
-    )
-
-    def product(left, right):
-        return lax.dot_general(
-            left, right, (((1,), (1,)), ((), ())), preferred_element_type=jnp.float32
-        )
-
-    gate_value = product(normed, expert_gate.reshape(-1, model_width))
-    up_value = product(normed, expert_up.reshape(-1, model_width))
-    hidden = jax.nn.silu(gate_value) * up_value
-    hidden = hidden.reshape(total, per_group, hidden_width) * share[:, :, None]
-    hidden = hidden.reshape(total, -1).astype(jnp.bfloat16)
-    own = lax.dynamic_slice_in_dim(normed, here * tokens, tokens, 0)
-    shared_hidden = (jax.nn.silu(product(own, shared_gate)) * product(own, shared_up)).astype(
-        jnp.bfloat16
-    )
-    shared_term = jnp.dot(shared_hidden, shared_down, preferred_element_type=jnp.float32)
-    term = jnp.dot(
-        hidden, expert_down.reshape(-1, model_width), preferred_element_type=jnp.float32
-    ).reshape(groups, tokens, model_width)
-    is_own = (jnp.arange(groups, dtype=jnp.int32) == here)[:, None, None]
-    term = (term + jnp.where(is_own, shared_term[None], 0.0)).astype(jnp.bfloat16)
-    blocks = (
-        term.reshape(groups, tokens, parts, slice_width)
-        .transpose(0, 2, 1, 3)
-        .reshape(groups * parts * tokens, slice_width)
-    )
-    return lax.psum_scatter(blocks, ("ep", "tp"), scatter_dimension=0, tiled=True)
+    params = pltpu.CompilerParams(vmem_limit_bytes=48 << 20)
+    whole = pl.BlockSpec(memory_space=VMEM)
+    normed = pl.pallas_call(
+        norm_kernel,
+        grid=(groups,),
+        in_specs=[pl.BlockSpec((parts, tokens, slice_width), lambda i: (i, 0, 0)), whole],
+        out_specs=pl.BlockSpec((tokens, model_width), lambda i: (i, 0)),
+        out_shape=jax.ShapeDtypeStruct((total, model_width), jnp.bfloat16),
+        cost_estimate=pl.CostEstimate(
+            flops=4 * total * model_width, bytes_accessed=4 * total * model_width, transcendentals=0
+        ),
+        name="norm",
+    )(gathered, ffn_gain[None])
+    weight_spec = pl.BlockSpec((1, hidden_width, model_width), lambda i: (i, 0, 0))
+    columns = per_group * hidden_width
+    hidden, shared_hidden = pl.pallas_call(
+        hidden_kernel,
+        grid=(per_group,),
+        in_specs=[whole, whole, whole, weight_spec, weight_spec, whole, whole],
+        out_specs=(
+            pl.BlockSpec((1, total, hidden_width), lambda i: (i, 0, 0)),
+            pl.BlockSpec((tokens, shared_width), lambda i: (0, 0)),
+        ),
+        out_shape=(
+            jax.ShapeDtypeStruct((per_group, total, hidden_width), jnp.bfloat16),
+            jax.ShapeDtypeStruct((tokens, shared_width), jnp.bfloat16),
+        ),
+        cost_estimate=pl.CostEstimate(
+            flops=4 * total * model_width * columns,
+            bytes_accessed=4 * columns * model_width,
+            transcendentals=total * columns,
+        ),
+        compiler_params=params,
+        name="hidden",
+    )(normed, all_routes, all_weights, expert_gate, expert_up, shared_gate, shared_up)
+    return pl.pallas_call(
+        down_kernel,
+        grid=(parts,),
+        in_specs=[
+            whole,
+            whole,
+            pl.BlockSpec((per_group, hidden_width, slice_width), lambda i: (0, 0, i)),
+            pl.BlockSpec((shared_width, slice_width), lambda i: (0, i)),
+        ],
+        out_specs=pl.BlockSpec((1, total, slice_width), lambda i: (i, 0, 0)),
+        out_shape=jax.ShapeDtypeStruct((parts, total, slice_width), jnp.bfloat16),
+        cost_estimate=pl.CostEstimate(
+            flops=2 * total * model_width * columns,
+            bytes_accessed=2 * (columns + total) * model_width,
+            transcendentals=0,
+        ),
+        compiler_params=params,
+        name="down",
+    )(hidden, shared_hidden, expert_down, shared_down)
+
+
+def combine_terms(term):
+    groups = lax.axis_size("ep")
+    _, total, slice_width = term.shape
+    tokens = total // groups
+    summed = lax.psum_scatter(term, "tp", scatter_dimension=0, tiled=True)
+    back = lax.all_to_all(
+        summed.reshape(groups, tokens, slice_width), "ep", split_axis=0, concat_axis=0, tiled=True
+    )
+    return jnp.sum(back.astype(jnp.float32), axis=0).astype(jnp.bfloat16)
 
 
 def on_device(
@@ -233,11 +342,16 @@
     shared_up,
     shared_down,
 ):
-    expert_out = experts_half(
-        moe_in,
+    rows, heads = cum_gate.shape
+    gathered = gather_tokens(moe_in)
+    got, packed = trade_rows(queries, keys, values, heads)
+    all_gates, all_routes, all_weights = trade_small(cum_gate, routes, route_weight)
+    gathered, got = lax.optimization_barrier((gathered, got))
+    term = expert_terms(
+        gathered,
         ffn_gain,
-        routes,
-        route_weight,
+        all_routes,
+        all_weights,
         expert_gate,
         expert_up,
         expert_down,
@@ -245,8 +359,9 @@
         shared_up,
         shared_down,
     )
-    mixed = attend(queries, keys, values, cum_gate, head_gain)
-    return (mixed, expert_out)
+    term, got = lax.optimization_barrier((term, got))
+    mixed = attend(got, packed, rows, all_gates, heads, head_gain)
+    return (mixed, combine_terms(term))
 
 
 def solution(mesh):

time: 302 us -> 219 us (0.73)
  blocking collectives: 68.7 us -> 16.4 us
  Pallas kernels: 31.5 us -> 67.9 us
  local copies, waits for them, and re-layouts: 44.7 us -> 10.9 us
  matrix products: 26.6 us -> 0 us
  other arithmetic: 14.5 us -> 4.02 us
  starting transfers between devices: 9.79 us -> 16.4 us
    all_gather x2 -> x0, blocking collectives: 54.5 us -> none  [the longest x1 28.1 us: experts_half(): all_routes = lax.all_gather(routes, 'ep', axis=0, tiled=True)]
    pallas_call x1 -> x4, Pallas kernels: 2.59 us -> 38.9 us  [the longest x1 15.7 us: expert_terms(): pl.pallas_call(hidden_kernel, grid=(per_group,), in_specs=[whole, whole,...]
    reduce_scatter x1, waiting for transfers between devices: 29.2 us -> 0.01 us  [combine_terms(): summed = lax.psum_scatter(term, 'tp', scatter_dimension=0, tiled=True)]
    dot_general x5 -> x0, matrix products: 26.6 us -> none  [the longest x3 18.1 us: product(): lax.dot_general(left, right, (((1,), (1,)), ((), ())), preferred_element_...]
    all_to_all x2 -> x3, waiting for transfers between devices: 54.2 us -> 73 us  [the longest x1 49 us: trade_rows(): lax.all_to_all(parcel, 'ep', split_axis=0, concat_axis=0, tiled=True)]
    convert_element_type x1, local copies, waits for them, and re-layouts: 10 us -> 0.12 us  [trade_small(): routes.astype(jnp.float32).reshape(-1)]
    all_gather x1, waiting for transfers between devices: 7.28 us -> 15.4 us  [gather_tokens(): return lax.all_gather(own_columns, ('ep', 'tp'), axis=0)]
    unnamed x34 -> x20, local copies, waits for them, and re-layouts: 12.9 us -> 4.85 us
  transfers between devices with their start and end apart: 4 -> 5, of which waited for: 4 -> 4; matrix products, arithmetic and copies ran while one was open for 5% -> 5% of each run, Pallas kernels for 10% -> 14%
where the time goes in v2:
time: 219 us; the launch traced here: 218 us
  waiting for transfers between devices  88.4 us (40%)
  Pallas kernels  67.9 us (31%)
  starting transfers between devices  16.4 us (7%)
  blocking collectives  16.4 us (7%)
  between operations  14.2 us (6%)
  local copies, waits for them, and re-layouts  10.9 us (5%)
  other arithmetic  4.02 us (2%)
    all_to_all x1, waiting for transfers between devices, trade_rows(): lax.all_to_all(parcel, 'ep', split_axis=0, concat_axis=0, tiled=True)  49 us
    pallas_call x1, Pallas kernels, attend(): pl.pallas_call(functools.partial(flash_kernel, splits, packed, rows), gri...  29 us
    all_to_all x1, waiting for transfers between devices, combine_terms(): lax.all_to_all(summed.reshape(groups, tokens, slice_width), 'ep', split_a...  23.4 us
    all_to_all x1, blocking collectives, attend(): back = lax.all_to_all(out, 'ep', split_axis=0, concat_axis=0, tiled=True)  16.4 us
    pallas_call x1, Pallas kernels, expert_terms(): pl.pallas_call(hidden_kernel, grid=(per_group,), in_specs=[whole, whole,...  15.7 us
    all_gather x1, waiting for transfers between devices, gather_tokens(): return lax.all_gather(own_columns, ('ep', 'tp'), axis=0)  15.4 us
    pallas_call x1, Pallas kernels, expert_terms(): pl.pallas_call(down_kernel, grid=(parts,), in_specs=[whole, whole, pl.Blo...  13 us
    pallas_call x1, Pallas kernels, expert_terms(): pl.pallas_call(norm_kernel, grid=(groups,), in_specs=[pl.BlockSpec((parts...  7.6 us
  transfers between devices with their start and end apart: 5, of which 4 were waited for; matrix products, arithmetic and copies ran while one was open for 5% of the time, Pallas kernels for 14%

profile of v2, /device:TPU:0, one launch (start us, length us, event | category | flops | bytes accessed | tf_op | source)
XLA Modules:
  0.0 218.2 jit_solution(5721029527298938819)
XLA Ops:
  7.2 1.0 copy-done
  8.2 0.7 constant_dynamic-slice_fusion
  8.9 0.7 convert_element_type.8
  9.6 0.1 copy.23
  9.7 0.1 reshape.41
  9.8 0.8 copy.24
  10.7 0.7 broadcast_in_dim.17
  11.5 0.7 all_to_all.18
  12.1 7.3 %all-to-all-start.1 = ((f32[8,1,1792]{2,1,0:T(1,128)}), f32[8,1,1792]{2,1,0:T(1,128)S(1)}, u32[]{:S(2)}, u32[]{:S(2)}) async-start(f32[8,1,1792]{2,1,0:T(1,128)} %all_to_all.18), calls=%async_computation.1 | async-start | bytes 114688 | tf_op jit(solution)/shard_map/all_to_all | solution.py:96
  19.4 2.6 %pack.1 = (bf16[4,768,128]{2,1,0:T(8,128)(2,1)}, bf16[8,192,128]{2,1,0:T(8,128)(2,1)}) custom-call(bf16[768,256]{1,0:T(8,128)(2,1)} %q_ref.1, bf16[768,256]{1,0:T(8,128)(2,1)} %k_ref.1, bf16[768,256]{1,0:T(8,128)(2,1)} %v_ref.1), custom_call_target="tpu_custom_call" | custom-call | tf_op jit(solution)/shard_map/pack/pallas_call | solution.py:113
  22.0 1.4 broadcast_in_dim.15
  23.4 2.4 %pad_maximum_fusion = bf16[8,960,128]{2,1,0:T(8,128)(2,1)} fusion(bf16[8,192,128]{2,1,0:T(8,128)(2,1)} %get-tuple-element.11, bf16[8,768,128]{2,1,0:T(8,128)(2,1)S(1)} %bitcast.15), kind=kLoop, calls=%fused_computation | loop fusion | flops 3932160 | bytes 3932160 | tf_op jit(solution)/shard_map/concatenate | solution.py:128
  25.8 0.6 all-to-all-done.1
  26.4 5.4 %all-to-all-start = ((bf16[8,960,128]{2,1,0:T(8,128)(2,1)}), bf16[8,960,128]{2,1,0:T(8,128)(2,1)S(1)}, u32[]{:S(2)}, u32[]{:S(2)}) async-start(bf16[8,960,128]{2,1,0:T(8,128)(2,1)} %pad_maximum_fusion), calls=%async_computation | async-start | bytes 3932160 | tf_op jit(solution)/shard_map/all_to_all | solution.py:129
  31.9 0.6 copy-done.6
  32.5 0.5 reshape.43.routes_ref
  33.0 0.5 reshape.44.weight_ref
  33.6 49.0 %all-to-all-done = bf16[8,960,128]{2,1,0:T(8,128)(2,1)S(1)} async-done(((bf16[8,960,128]{2,1,0:T(8,128)(2,1)}), bf16[8,960,128]{2,1,0:T(8,128)(2,1)S(1)}, u32[]{:S(2)}, u32[]{:S(2)}) %all-to-all-start) | async-done | bytes 1966112 | tf_op jit(solution)/shard_map/all_to_all | solution.py:129
  82.6 15.4 %all-gather.3.cloned.1.call-done = bf16[4096,512]{1,0:T(8,128)(2,1)} async-done(((bf16[128,512]{1,0:T(8,128)(2,1)}), bf16[4096,512]{1,0:T(8,128)(2,1)}) %all-gather.3.cloned.1.call-update) | async-done | bytes 4194320 | tf_op jit(solution)/shard_map/all_gather | solution.py:238
  98.0 7.6 %norm.1.x_ref = bf16[1024,2048]{1,0:T(8,128)(2,1)} custom-call(bf16[32,128,512]{2,1,0:T(8,128)(2,1)} %bitcast.16, f32[1,2048]{1,0:T(1,128)} %bitcast.22), custom_call_target="tpu_custom_call" | custom-call | flops 8388608 | bytes 8388608 | tf_op jit(solution)/shard_map/norm/pallas_call | solution.py:263
  105.6 15.7 %hidden.1 = (bf16[4,1024,256]{2,1,0:T(8,128)(2,1)S(1)}, bf16[128,128]{1,0:T(8,128)(2,1)S(1)}) custom-call(bf16[1024,2048]{1,0:T(8,128)(2,1)} %norm.1.x_ref, s32[1024,4]{1,0:T(8,128)S(1)} %reshape.43.routes_ref, f32[1024,4]{1,0:T(8,128)S(1)} %reshape.44.weight_ref, bf16[4,256,2048]{2,1,0:T(8,128)(2,1)} %gate_ref.1, bf16[4,256,2048]{2,1,0:T(8,128)(2,1)} %up_ref.1, ...), custom_call_target="tpu_custom_call" | custom-call | flops 8589934592 | bytes 8388608 | tf_op jit(solution)/shard_map/hidden/pallas_call | solution.py:276
  121.4 13.0 %down.1 = bf16[4,1024,512]{2,1,0:T(8,128)(2,1)} custom-call(bf16[4,1024,256]{2,1,0:T(8,128)(2,1)S(1)} %get-tuple-element.13.hid_ref, bf16[128,128]{1,0:T(8,128)(2,1)S(1)} %get-tuple-element.14.shid_ref, bf16[4,256,2048]{2,1,0:T(8,128)(2,1)} %down_ref.1, bf16[128,2048]{1,0:T(8,128)(2,1)S(1)} %copy-done.3), custom_call_target="tpu_custom_call" | custom-call | flops 4294967296 | bytes 8388608 | tf_op jit(solution)/shard_map/down/pallas_call | solution.py:296
  134.4 0.6 copy-done.7
  135.2 0.7 slice.22
  136.1 29.0 %flash.1 = bf16[8,192,128]{2,1,0:T(8,128)(2,1)S(1)} custom-call(bf16[8,192,128]{2,1,0:T(8,128)(2,1)S(1)} %slice.17.q_ref, bf16[6144,128]{1,0:T(8,128)(2,1)S(1)} %bitcast.14, f32[8,1,768]{2,1,0:T(1,128)S(1)} %reshape.46.gate_ref, f32[1,128]{1,0:T(1,128)S(1)} %maximum_bitcast_fusion.gain_ref), custom_call_target="tpu_custom_call" | custom-call | flops 5435817984 | bytes 3145728 | tf_op jit(solution)/shard_map/flash/pallas_call | solution.py:145
  165.1 16.4 %all_to_all.27 = bf16[8,192,128]{2,1,0:T(8,128)(2,1)S(1)} all-to-all(bf16[8,192,128]{2,1,0:T(8,128)(2,1)S(1)} %flash.1), channel_id=1, replica_groups=mesh['ep'=8,'tp'=4] {'ep'}, dimensions={0} | all-to-all | bytes 786432 | tf_op jit(solution)/shard_map/all_to_all | solution.py:162
  181.5 3.6 %all-to-all-start.3 = ((bf16[8,128,512]{2,1,0:T(8,128)(2,1)}), bf16[8,128,512]{2,1,0:T(8,128)(2,1)S(1)}, u32[]{:S(2)}, u32[]{:S(2)}) async-start(bf16[8,128,512]{2,1,0:T(8,128)(2,1)} %bitcast.18), calls=%async_computation.4 | async-start | bytes 2097152 | tf_op jit(solution)/shard_map/all_to_all | solution.py:322
  185.0 0.2 copy.25
  185.3 0.6 copy.28
  185.8 1.2 reshape.51
  187.1 23.4 %all-to-all-done.3 = bf16[8,128,512]{2,1,0:T(8,128)(2,1)S(1)} async-done(((bf16[8,128,512]{2,1,0:T(8,128)(2,1)}), bf16[8,128,512]{2,1,0:T(8,128)(2,1)S(1)}, u32[]{:S(2)}, u32[]{:S(2)}) %all-to-all-start.3) | async-done | bytes 1048608 | tf_op jit(solution)/shard_map/all_to_all | solution.py:322
  210.5 0.8 reduce_sum.12
  (29 shorter events, 0.6 us)
Async XLA Ops:
  7.2 1.0 copy-start
  7.2 90.8 %all-gather.3.cloned.1.call-start = ((), (), s32[]{:S(2)}) async-start(), calls=%async_computation.6 | async-start | bytes 4325376 | tf_op jit(solution)/shard_map/all_gather | solution.py:238
  12.1 14.2 %all-to-all-start.1 = ((f32[8,1,1792]{2,1,0:T(1,128)}), f32[8,1,1792]{2,1,0:T(1,128)S(1)}, u32[]{:S(2)}, u32[]{:S(2)}) async-start(f32[8,1,1792]{2,1,0:T(1,128)} %all_to_all.18), calls=%async_computation.1 | async-start | bytes 114688 | tf_op jit(solution)/shard_map/all_to_all | solution.py:96
  26.4 56.2 %all-to-all-start = ((bf16[8,960,128]{2,1,0:T(8,128)(2,1)}), bf16[8,960,128]{2,1,0:T(8,128)(2,1)S(1)}, u32[]{:S(2)}, u32[]{:S(2)}) async-start(bf16[8,960,128]{2,1,0:T(8,128)(2,1)} %pad_maximum_fusion), calls=%async_computation | async-start | bytes 3932160 | tf_op jit(solution)/shard_map/all_to_all | solution.py:129
  31.8 149.7 %reduce-scatter.2.cloned.1.call-start = ((), (), s32[]{:S(2)}) async-start(), calls=%async_computation.5 | async-start | bytes 5242880 | tf_op jit(solution)/shard_map/reduce_scatter | solution.py:321
  31.9 0.6 copy-start.6
  82.6 15.4 %copy-start.4 = (bf16[8,960,128]{2,1,0:T(8,128)(2,1)}, bf16[8,960,128]{2,1,0:T(8,128)(2,1)S(1)}, u32[]{:S(2)}) copy-start(bf16[8,960,128]{2,1,0:T(8,128)(2,1)S(1)} %all-to-all-done) | copy-start | bytes 5898244
  98.0 7.6 %copy-start.1 = (bf16[128,2048]{1,0:T(8,128)(2,1)S(1)}, bf16[128,2048]{1,0:T(8,128)(2,1)}, u32[]{:S(2)}) copy-start(bf16[128,2048]{1,0:T(8,128)(2,1)} %sgate_ref.1) | copy-start | bytes 1572868
  98.0 7.6 %copy-start.2 = (bf16[128,2048]{1,0:T(8,128)(2,1)S(1)}, bf16[128,2048]{1,0:T(8,128)(2,1)}, u32[]{:S(2)}) copy-start(bf16[128,2048]{1,0:T(8,128)(2,1)} %sup_ref.1) | copy-start | bytes 1572868
  105.6 15.8 %copy-start.3 = (bf16[128,2048]{1,0:T(8,128)(2,1)S(1)}, bf16[128,2048]{1,0:T(8,128)(2,1)}, u32[]{:S(2)}) copy-start(bf16[128,2048]{1,0:T(8,128)(2,1)} %sdown_ref.1) | copy-start | bytes 1572868
  134.4 0.7 copy-start.7
  134.4 1.6 copy-start.5
  181.5 29.0 %all-to-all-start.3 = ((bf16[8,128,512]{2,1,0:T(8,128)(2,1)}), bf16[8,128,512]{2,1,0:T(8,128)(2,1)S(1)}, u32[]{:S(2)}, u32[]{:S(2)}) async-start(bf16[8,128,512]{2,1,0:T(8,128)(2,1)} %bitcast.18), calls=%async_computation.4 | async-start | bytes 2097152 | tf_op jit(solution)/shard_map/all_to_all | solution.py:322
Sparse Core Ops, SparseCore 0:
  11.4 86.5 all-gather.2
  134.5 43.3 reduce-scatter.1
